TPU v7x, 32 devices: a whole 2x2x4 slice. The times are simulated.
32 devices in a mesh: sp: 8 (over z, x), tp: 4 (over y, core).
Axes of the slice: x: 2, y: 2, z: 4, core: 2. Of those that a mesh axis runs over, the one named last changes fastest.
Arguments:
- x_resid: bfloat16 [1024, 2048], P(('sp', 'tp')), may hold values from -3 to 3
- query_proj: bfloat16 [1024, 2048], P('sp', 'tp'), may hold values from -6 to 6
- projected_key_heads: bfloat16 [1024, 1024], P('sp', 'tp'), may hold values from -6 to 6
- projected_value_heads: bfloat16 [1024, 1024], P('sp', 'tp'), may hold values from -6 to 6
- query_gain: float32 [128], replicated, may hold values from 1.3 to 6.5
- key_norm_gain: float32 [128], replicated, may hold values from 1.3 to 6.5
- out_weight: bfloat16 [2048, 2048], P('tp'), may hold values from -0.125 to 0.125
- ffn_gain: float32 [2048], replicated, may hold values from 0.1 to 1.9
- routing: int32 [1024, 2], P(('sp', 'tp')), may hold values from 0 to 7, all different within a row; in each aligned block of 32 rows (0 to 31, 32 to 63, ...) at most 16 rows name the same one
- route_scores: float32 [1024, 2], P(('sp', 'tp')), may hold values from -6 to 6
- expert_gate: bfloat16 [8, 2048, 4096], P('sp', None, 'tp'), may hold values from -0.125 to 0.125
- expert_up: bfloat16 [8, 2048, 4096], P('sp', None, 'tp'), may hold values from -0.125 to 0.125
- expert_down: bfloat16 [8, 4096, 2048], P('sp', 'tp'), may hold values from -0.09375 to 0.09375
Outputs:
- layer_out: bfloat16 [1024, 2048], P(('sp', 'tp'))
Inputs may be any that keep to these rules, and one draw needn't show every extreme that they name: `routing`: each row names 2 different experts. In each aligned block of 32 rows (the rows of one device) no expert is named by more than 16 rows, a bound that some block reaches.
All inputs are finite; a program needn't handle non-finite values.
Results may differ from a plain program's by a relative error of at most 0.018.
The roundings to bfloat16 on the way count: a program that leaves them out, or rounds other values in their place, can miss the bound.
Values may be sent and summed in bfloat16 or wider, within the bound.
A program may use at most 128 MiB of HBM per device.

v0:
```python
import functools
import math

import jax
import jax.numpy as jnp
import numpy as np
from jax import lax
from jax.experimental import pallas as pl
from jax.experimental.pallas import tpu as pltpu
from jax.sharding import PartitionSpec as P

MESH = pl.DeviceIdType.MESH

HEAD_WIDTH = 128
TOP = 2
GRID_W = 64


NORM_EPS = 1e-06
ROPE_BASE = 10000.0
NEG_LARGE = -1e30


def rms_scale(values, norm_gain):
    return (
        values * lax.rsqrt(jnp.mean(values * values, axis=-1, keepdims=True) + NORM_EPS) * norm_gain
    )


def grid_angles(token_positions, head_size):
    freq_count = head_size // 4
    frequency = ROPE_BASE ** (-jnp.arange(freq_count, dtype=jnp.float32) / freq_count)
    grid_row = (token_positions // GRID_W).astype(jnp.float32)
    grid_col = (token_positions % GRID_W).astype(jnp.float32)
    return (grid_row[:, None] * frequency, grid_col[:, None] * frequency)


def turn_half(values, angles):
    cosine = jnp.cos(angles)[:, None, :]
    sine_part = jnp.sin(angles)[:, None, :]
    leading, trailing = jnp.split(values, 2, axis=-1)
    return jnp.concatenate(
        [leading * cosine - trailing * sine_part, trailing * cosine + leading * sine_part], axis=-1
    )


def normalize_rotate(projected, norm_gain, token_positions, heads):
    length = projected.shape[0]
    values = projected.astype(jnp.float32).reshape(length, heads, -1)
    head_size = values.shape[-1]
    values = rms_scale(values, norm_gain)
    row_angle, col_angle = grid_angles(token_positions, head_size)
    half_size = head_size // 2
    turned = jnp.concatenate(
        [
            turn_half(values[..., :half_size], row_angle),
            turn_half(values[..., half_size:], col_angle),
        ],
        axis=-1,
    )
    return turned.reshape(length, heads * head_size).astype(jnp.bfloat16)


def local_plain(
    x_resid,
    query_proj,
    projected_key_heads,
    projected_value_heads,
    query_gain,
    key_norm_gain,
    out_weight,
    ffn_gain,
    routing,
    route_scores,
    expert_gate,
    expert_up,
    expert_down,
):
    seq_rows = query_proj.shape[0]
    q_heads = query_proj.shape[1] // HEAD_WIDTH
    kv_heads = projected_key_heads.shape[1] // HEAD_WIDTH
    head_groups = q_heads // kv_heads
    token_positions = lax.axis_index("sp") * seq_rows + jnp.arange(seq_rows, dtype=jnp.int32)
    query_rows = normalize_rotate(query_proj, query_gain, token_positions, q_heads)
    rotated_key_rows = normalize_rotate(
        projected_key_heads, key_norm_gain, token_positions, kv_heads
    )
    query_grid = query_rows.reshape(seq_rows, kv_heads, head_groups, HEAD_WIDTH)
    score_scale = HEAD_WIDTH ** (-0.5)
    run_max = jnp.full((kv_heads, head_groups, seq_rows), NEG_LARGE, jnp.float32)
    key_piece = lax.all_gather(rotated_key_rows, "sp", axis=0, tiled=True).reshape(
        -1, kv_heads, HEAD_WIDTH
    )
    value_piece = lax.all_gather(projected_value_heads, "sp", axis=0, tiled=True).reshape(
        -1, kv_heads, HEAD_WIDTH
    )
    scores = (
        jnp.einsum("qhgd,khd->hgqk", query_grid, key_piece, preferred_element_type=jnp.float32)
        * score_scale
    )
    new_max = jnp.maximum(run_max, jnp.max(scores, axis=-1))
    weights = jnp.exp(scores - new_max[..., None])
    new_total = jnp.sum(weights, axis=-1)
    addition = jnp.einsum(
        "hgqk,khd->hgqd",
        weights.astype(jnp.bfloat16),
        value_piece,
        preferred_element_type=jnp.float32,
    )
    attended = (
        (addition / new_total[..., None])
        .transpose(2, 0, 1, 3)
        .reshape(seq_rows, q_heads * HEAD_WIDTH)
        .astype(jnp.bfloat16)
    )
    own_tokens = x_resid.shape[0]
    model_width = x_resid.shape[1]
    row_block = attended
    attn_proj = lax.psum_scatter(
        jnp.dot(row_block, out_weight, preferred_element_type=jnp.float32).astype(jnp.bfloat16),
        "tp",
        scatter_dimension=0,
        tiled=True,
    )
    middle = x_resid.astype(jnp.float32) + attn_proj.astype(jnp.float32)
    normed = rms_scale(middle, ffn_gain).astype(jnp.bfloat16)
    experts_all = lax.axis_size("sp") * expert_gate.shape[0]
    capacity = max(2, 2 * own_tokens * TOP // experts_all)
    flat_expert = routing.reshape(-1)
    one_hot = (flat_expert[:, None] == jnp.arange(experts_all, dtype=jnp.int32)[None, :]).astype(
        jnp.int32
    )
    earlier = jnp.cumsum(one_hot, axis=0) - one_hot
    slot_rank = jnp.sum(earlier * one_hot, axis=1)
    target = flat_expert * capacity + slot_rank
    chooser = (
        jnp.arange(experts_all * capacity, dtype=jnp.int32)[:, None] == target[None, :]
    ).astype(jnp.float32)
    gate_share = jax.nn.softmax(route_scores, axis=-1).reshape(-1)
    picker = jnp.sum(chooser.reshape(experts_all * capacity, own_tokens, TOP), axis=2).astype(
        jnp.bfloat16
    )
    combiner = jnp.sum(
        (chooser * gate_share[None, :]).reshape(experts_all * capacity, own_tokens, TOP), axis=2
    )
    dispatch = (
        jnp.dot(picker, normed, preferred_element_type=jnp.float32)
        .astype(jnp.bfloat16)
        .reshape(experts_all, capacity, model_width)
    )
    gate_matrix = expert_gate[0]
    up_matrix = expert_up[0]
    down_matrix = expert_down[0]
    arrived = lax.all_to_all(dispatch, "sp", split_axis=0, concat_axis=0, tiled=True)
    row_block = lax.all_gather(arrived.reshape(-1, model_width), "tp", axis=0, tiled=True)
    gate_part = jnp.dot(row_block, gate_matrix, preferred_element_type=jnp.float32)
    up_part = jnp.dot(row_block, up_matrix, preferred_element_type=jnp.float32)
    hidden = (jax.nn.silu(gate_part) * up_part).astype(jnp.bfloat16)
    row_block = hidden
    expert_result = lax.psum_scatter(
        jnp.dot(row_block, down_matrix, preferred_element_type=jnp.float32).astype(jnp.bfloat16),
        "tp",
        scatter_dimension=0,
        tiled=True,
    )
    returned = lax.all_to_all(
        expert_result.reshape(-1, capacity, model_width),
        "sp",
        split_axis=0,
        concat_axis=0,
        tiled=True,
    )
    routed = jnp.einsum(
        "st,sd->td",
        combiner,
        returned.reshape(-1, model_width).astype(jnp.float32),
        precision=lax.Precision.HIGHEST,
    )
    return (middle + routed).astype(jnp.bfloat16)


def rdma(src, dst, send_sem, recv_sem, device):
    return pltpu.make_async_remote_copy(
        src_ref=src,
        dst_ref=dst,
        send_sem=send_sem,
        recv_sem=recv_sem,
        device_id=device,
        device_id_type=MESH,
    )


def turn_head(values, gain, cosine, sine):
    values = values * lax.rsqrt(jnp.mean(values * values, axis=-1, keepdims=True) + NORM_EPS) * gain
    width = values.shape[1]
    quarter = width // 4
    lane = lax.broadcasted_iota(jnp.int32, values.shape, 1)
    swapped = jnp.where(
        lane % (2 * quarter) < quarter,
        pltpu.roll(values, width - quarter, 1),
        pltpu.roll(values, quarter, 1),
    )
    return (values * cosine + swapped * sine).astype(jnp.bfloat16)


def flip(index, mask):
    bit = 1
    while bit <= mask:
        if mask // bit % 2:
            index = index + bit * (1 - 2 * (index // bit % 2))
        bit = bit * 2
    return index


def hop_order(count):
    half, quarter = count // 2, count // 4
    near, far = list(range(half)), list(range(half, count))
    return near[:quarter] + far + near[quarter:]


def layer_kernel(
    n_sp,
    n_tp,
    capacity,
    q_ref,
    k_ref,
    v_ref,
    freq_ref,
    qg_ref,
    kg_ref,
    x_ref,
    fg_ref,
    route_ref,
    score_ref,
    ow_hbm,
    wg_hbm,
    wu_hbm,
    wd_hbm,
    out_ref,
    kbuf,
    vbuf,
    qs,
    att,
    part,
    rsbuf,
    mid,
    disp,
    rows,
    hid,
    eo,
    cor,
    pair,
    yrec,
    res,
    ret,
    ow,
    wg,
    wu,
    wd,
    w_sem,
    k_s,
    k_r,
    v_s,
    v_r,
    rs_s,
    rs_r,
    d_s,
    rows_r,
    y_s,
    c_s,
    e_s,
    e_r,
    p_s,
    p_r,
    b_s,
    b_r,
):
    s = lax.axis_index("sp")
    t = lax.axis_index("tp")
    n_x = math.isqrt(n_sp // 2)
    if n_x == 0 or n_sp % n_x:
        n_x = 1
    n_z = n_sp // n_x
    n_y = n_tp // 2
    y, c = t // 2, t % 2
    core_peer = (s, y * 2 + 1 - c)
    order = hop_order(n_sp)
    seq_rows, q_width = q_ref.shape
    kv_width = k_ref.shape[1]
    q_heads, kv_heads = q_width // HEAD_WIDTH, kv_width // HEAD_WIDTH
    groups = q_heads // kv_heads
    own, model = x_ref.shape
    f_width = wg.shape[1]
    pending = []

    def send(src, dst, send_sem, recv_sem, device):
        copy = rdma(src, dst, send_sem, recv_sem, device)
        copy.start()
        pending.append(copy)

    def arrive(dst, recv_sem):
        rdma(dst, dst, recv_sem, recv_sem, core_peer).wait_recv()

    weight_copies = [
        pltpu.make_async_copy(ow_hbm, ow, w_sem.at[0]),
        pltpu.make_async_copy(wg_hbm.at[0], wg, w_sem.at[1]),
        pltpu.make_async_copy(wu_hbm.at[0], wu, w_sem.at[2]),
        pltpu.make_async_copy(wd_hbm.at[0], wd, w_sem.at[3]),
    ]
    for copy in weight_copies:
        copy.start()

    barrier = pltpu.get_barrier_semaphore()
    for d in range(1, n_sp):
        pl.semaphore_signal(barrier, inc=1, device_id=((s + d) % n_sp, t), device_id_type=MESH)
    for d in range(1, n_tp):
        pl.semaphore_signal(barrier, inc=1, device_id=(s, (t + d) % n_tp), device_id_type=MESH)

    table = (seq_rows, HEAD_WIDTH)
    place = lax.broadcasted_iota(jnp.int32, table, 0) + s * seq_rows
    column = lax.broadcasted_iota(jnp.int32, table, 1)
    step = jnp.where(column < HEAD_WIDTH // 2, place // GRID_W, place % GRID_W)
    angles = step.astype(jnp.float32) * freq_ref[...]
    cosine, sine = jnp.cos(angles), jnp.sin(angles)
    sine = jnp.where(column % (HEAD_WIDTH // 2) < HEAD_WIDTH // 4, -sine, sine)
    for h in range(kv_heads):
        cols = slice(h * HEAD_WIDTH, (h + 1) * HEAD_WIDTH)
        kbuf[0, :, cols] = turn_head(k_ref[:, cols].astype(jnp.float32), kg_ref[...], cosine, sine)
    pl.semaphore_wait(barrier, n_sp - 1 + n_tp - 1)

    for slot in list(range(1, n_x)) + list(range(n_x, n_sp, n_x)):
        send(kbuf.at[0], kbuf.at[slot], k_s.at[slot], k_r.at[slot], (flip(s, slot), t))

    def send_values(slot):
        send(v_ref, vbuf.at[slot], v_s.at[slot], v_r.at[slot], (flip(s, slot), t))

    for slot in range(1, n_x):
        send_values(slot)
    vbuf[0] = v_ref[...]
    for h in range(q_heads):
        cols = slice(h * HEAD_WIDTH, (h + 1) * HEAD_WIDTH)
        kv, member = h // groups, h % groups
        qs[kv, member * seq_rows : (member + 1) * seq_rows, :] = turn_head(
            q_ref[:, cols].astype(jnp.float32), qg_ref[...], cosine, sine
        )
    total_slots = n_sp * capacity
    slot_at = lax.broadcasted_iota(jnp.int32, (total_slots, own), 0)
    slot_place = slot_at // capacity
    slot_expert = jnp.zeros_like(slot_at)
    for k, d in enumerate(order):
        slot_expert = jnp.where(slot_place == k, flip(s, d), slot_expert)
    first_hit = route_ref[0:1, :] == slot_expert
    named = first_hit | (route_ref[1:2, :] == slot_expert)
    earlier = (
        lax.broadcasted_iota(jnp.int32, (own, own), 0)
        < lax.broadcasted_iota(jnp.int32, (own, own), 1)
    )
    rank = jnp.dot(
        named.astype(jnp.float32).astype(jnp.bfloat16),
        earlier.astype(jnp.float32).astype(jnp.bfloat16),
        preferred_element_type=jnp.float32,
    )
    picked = jnp.where(
        named & (rank == (slot_at % capacity).astype(jnp.float32)), 1.0, 0.0
    )
    route_scores = score_ref[...]
    share = jnp.exp(route_scores - jnp.max(route_scores, axis=0, keepdims=True))
    share = share / jnp.sum(share, axis=0, keepdims=True)
    combiner = picked * jnp.where(first_hit, share[0:1, :], share[1:2, :])
    picker = picked.astype(jnp.bfloat16)

    for buf, s_sem, r_sem in ((kbuf, k_s, k_r), (vbuf, v_s, v_r)):
        for dz in range(1, n_z):
            slot = dz * n_x
            arrive(buf.at[slot], r_sem.at[slot])
            for dx in range(1, n_x):
                send(
                    buf.at[slot],
                    buf.at[slot + dx],
                    s_sem.at[slot + dx],
                    r_sem.at[slot + dx],
                    (flip(s, dx), t),
                )
            if buf is kbuf:
                send_values(slot)
    for slot in range(n_sp):
        if slot % n_x:
            arrive(kbuf.at[slot], k_r.at[slot])
    keys_all = n_sp * seq_rows
    score_scale = HEAD_WIDTH ** (-0.5)
    heads_done = []
    for kv in range(kv_heads):
        cols = slice(kv * HEAD_WIDTH, (kv + 1) * HEAD_WIDTH)
        keys = kbuf[:, :, cols].reshape(keys_all, HEAD_WIDTH)
        scores = (
            lax.dot_general(
                qs[kv], keys, (((1,), (1,)), ((), ())), preferred_element_type=jnp.float32
            )
            * score_scale
        )
        weights = jnp.exp(scores - jnp.max(scores, axis=-1, keepdims=True))
        total = jnp.sum(weights, axis=-1, keepdims=True)
        heads_done.append((weights.astype(jnp.bfloat16), total))
    for slot in range(n_sp):
        if slot % n_x:
            arrive(vbuf.at[slot], v_r.at[slot])
    for kv in range(kv_heads):
        cols = slice(kv * HEAD_WIDTH, (kv + 1) * HEAD_WIDTH)
        values = vbuf[:, :, cols].reshape(keys_all, HEAD_WIDTH)
        weights, total = heads_done[kv]
        mixed = jnp.dot(weights, values, preferred_element_type=jnp.float32) / total
        for member in range(groups):
            h = kv * groups + member
            att[:, h * HEAD_WIDTH : (h + 1) * HEAD_WIDTH] = mixed[
                member * seq_rows : (member + 1) * seq_rows
            ].astype(jnp.bfloat16)

    weight_copies[0].wait()
    tile = min(512, model)
    for j in range(model // tile):
        cols = slice(j * tile, (j + 1) * tile)
        part[:, :, cols] = (
            jnp.dot(att[...], ow[:, cols], preferred_element_type=jnp.float32)
            .astype(jnp.bfloat16)
            .reshape(n_tp, own, tile)
        )
    for d in range(n_tp - 1, 0, -1):
        peer = flip(t, d)
        send(part.at[peer], rsbuf.at[d], rs_s.at[d], rs_r.at[d], (s, peer))
    summed = part[t].astype(jnp.float32)
    for d in range(1, n_tp):
        arrive(rsbuf.at[d], rs_r.at[d])
        summed = summed + rsbuf[d].astype(jnp.float32)
    middle = x_ref[...].astype(jnp.float32) + summed.astype(jnp.bfloat16).astype(jnp.float32)
    mid[...] = middle
    normed = (
        middle
        * lax.rsqrt(jnp.mean(middle * middle, axis=-1, keepdims=True) + NORM_EPS)
        * fg_ref[...]
    ).astype(jnp.bfloat16)
    chosen = (
        jnp.dot(picker, normed, preferred_element_type=jnp.float32)
        .astype(jnp.bfloat16)
        .reshape(n_sp, capacity, model)
    )
    disp[...] = chosen

    def dispatch(k):
        send(disp.at[k], rows.at[k, t], d_s.at[k], rows_r.at[k, t], (flip(s, order[k]), t))

    window = n_sp // 2
    for k in range(1, window):
        dispatch(k)
    rows[0, t] = chosen[0]

    def forward(k):
        if k:
            arrive(rows.at[k, t], rows_r.at[k, t])
        for dy in range(1, n_y):
            peer = ((y + dy) % n_y) * 2 + c
            send(rows.at[k, t], rows.at[k, t], y_s.at[k, dy], rows_r.at[k, t], (s, peer))
        send(rows.at[k, t], rows.at[k, t], c_s.at[k, 0], rows_r.at[k, t], core_peer)

    def relay(k):
        for dy in range(1, n_y):
            source = ((y + n_y - dy) % n_y) * 2 + c
            arrive(rows.at[k, source], rows_r.at[k, source])
            send(
                rows.at[k, source],
                rows.at[k, source],
                c_s.at[k, dy],
                rows_r.at[k, source],
                core_peer,
            )

    def settle(k):
        for dy in range(n_y):
            source = ((y + n_y - dy) % n_y) * 2 + 1 - c
            arrive(rows.at[k, source], rows_r.at[k, source])

    n_groups = 2
    group = n_sp // n_groups
    group_rows = group * n_tp * capacity

    def give_pair(g):
        ks = pl.ds(g * group, group)
        send(eo.at[1 - c, :, ks], cor.at[:, ks], e_s.at[g], e_r.at[g], core_peer)

    def sum_pair(k):
        for dy in range(1, n_y):
            far = (y + dy) % n_y
            pair[dy, k] = (
                eo[c, far, k].astype(jnp.float32) + cor[far, k].astype(jnp.float32)
            ).astype(jnp.bfloat16)
            send(pair.at[dy, k], yrec.at[dy, k], p_s.at[k, dy], p_r.at[k, dy], (s, far * 2 + c))

    def start_pairs(g, slots):
        arrive(cor.at[:, pl.ds(g * group, group)], e_r.at[g])
        for k in slots[:2]:
            sum_pair(k)

    def return_next(i, slots):
        give_back(slots[i])
        if i + 2 < len(slots):
            sum_pair(slots[i + 2])

    def give_back(k):
        whole = eo[c, y, k].astype(jnp.float32) + cor[y, k].astype(jnp.float32)
        for dy in range(1, n_y):
            arrive(yrec.at[dy, k], p_r.at[k, dy])
            whole = whole + yrec[dy, k].astype(jnp.float32)
        if k == 0:
            ret[0] = whole.astype(jnp.bfloat16)
        else:
            res[k] = whole.astype(jnp.bfloat16)
            send(res.at[k], ret.at[k], b_s.at[k], b_r.at[k], (flip(s, order[k]), t))

    def experts(g, hooks):
        hooks = list(hooks)
        block = rows[g * group : (g + 1) * group].reshape(group_rows, model)
        f_tile = min(256, f_width)
        for j in range(f_width // f_tile):
            cols = slice(j * f_tile, (j + 1) * f_tile)
            gate = jnp.dot(block, wg[:, cols], preferred_element_type=jnp.float32)
            up = jnp.dot(block, wu[:, cols], preferred_element_type=jnp.float32)
            hid[:, cols] = (gate / (1.0 + jnp.exp(-gate)) * up).astype(jnp.bfloat16)
            if hooks:
                hooks.pop(0)()
        if g == 0:
            weight_copies[3].wait()
        for j in range(model // tile):
            cols = slice(j * tile, (j + 1) * tile)
            down = jnp.dot(hid[...], wd[:, cols], preferred_element_type=jnp.float32)
            down = down.astype(jnp.bfloat16).reshape(group, n_y, 2, capacity, tile)
            for core in range(2):
                for far in range(n_y):
                    eo[core, far, g * group : (g + 1) * group, :, cols] = down[:, far, core]
            if hooks:
                hooks.pop(0)()
        for hook in hooks:
            hook()

    for k in range(group):
        forward(k)
        if k:
            dispatch(window + k - 1)
    dispatch(n_sp - 1)
    for k in range(group):
        relay(k)
    for k in range(group):
        settle(k)
    weight_copies[1].wait()
    weight_copies[2].wait()
    late = range(group, n_sp)
    experts(
        0,
        [functools.partial(forward, k) for k in late] + [functools.partial(relay, k) for k in late],
    )
    give_pair(0)
    for k in late:
        settle(k)
    nothing = lambda: None
    early = list(range(group - 1, -1, -1))
    experts(
        1,
        [functools.partial(start_pairs, 0, early), nothing, nothing, nothing]
        + [functools.partial(return_next, i, early) for i in range(group)],
    )
    give_pair(1)
    start_pairs(1, late)
    for i in range(group):
        return_next(i, late)
    for k in range(1, n_sp):
        arrive(ret.at[k], b_r.at[k])
    high = combiner.astype(jnp.bfloat16)
    rest = combiner - high.astype(jnp.float32)
    middle_part = rest.astype(jnp.bfloat16)
    low = (rest - middle_part.astype(jnp.float32)).astype(jnp.bfloat16)
    returned = ret[...].reshape(total_slots, model)
    routed = jnp.zeros((own, model), jnp.float32)
    for piece in (high, middle_part, low):
        routed = routed + lax.dot_general(
            piece, returned, (((0,), (0,)), ((), ())), preferred_element_type=jnp.float32
        )
    out_ref[...] = mid[...] + routed
    for copy in pending:
        copy.wait_send()


def head_frequency():
    quarter = HEAD_WIDTH // 4
    frequency = ROPE_BASE ** (-np.arange(quarter, dtype=np.float32) / quarter)
    return jnp.asarray(np.tile(frequency, 4).reshape(1, HEAD_WIDTH), jnp.float32)


def local(
    x_resid,
    query_proj,
    projected_key_heads,
    projected_value_heads,
    query_gain,
    key_norm_gain,
    out_weight,
    ffn_gain,
    routing,
    route_scores,
    expert_gate,
    expert_up,
    expert_down,
):
    n_sp, n_tp = lax.axis_size("sp"), lax.axis_size("tp")
    own, model = x_resid.shape
    experts_all = n_sp * expert_gate.shape[0]
    capacity = max(2, 2 * own * TOP // experts_all)
    if capacity % 16 or n_tp & (n_tp - 1) or n_sp & (n_sp - 1) or n_tp < 2 or n_sp < 4 or expert_gate.shape[0] != 1:
        return local_plain(
            x_resid,
            query_proj,
            projected_key_heads,
            projected_value_heads,
            query_gain,
            key_norm_gain,
            out_weight,
            ffn_gain,
            routing,
            route_scores,
            expert_gate,
            expert_up,
            expert_down,
        )
    seq_rows, q_width = query_proj.shape
    kv_width = projected_key_heads.shape[1]
    kv_heads = kv_width // HEAD_WIDTH
    groups = q_width // kv_width
    f_width = expert_gate.shape[2]
    n_y = n_tp // 2
    bf16 = jnp.bfloat16
    dma = pltpu.SemaphoreType.DMA
    vmem = pl.BlockSpec(memory_space=pltpu.VMEM)
    hbm = pl.BlockSpec(memory_space=pl.ANY)
    return pl.pallas_call(
        functools.partial(layer_kernel, n_sp, n_tp, capacity),
        out_shape=jax.ShapeDtypeStruct((own, model), jnp.float32),
        in_specs=[vmem] * 10 + [hbm] * 4,
        out_specs=vmem,
        scratch_shapes=[
            pltpu.VMEM((n_sp, seq_rows, kv_width), bf16),
            pltpu.VMEM((n_sp, seq_rows, kv_width), bf16),
            pltpu.VMEM((kv_heads, groups * seq_rows, HEAD_WIDTH), bf16),
            pltpu.VMEM((seq_rows, q_width), bf16),
            pltpu.VMEM((n_tp, own, model), bf16),
            pltpu.VMEM((n_tp, own, model), bf16),
            pltpu.VMEM((own, model), jnp.float32),
            pltpu.VMEM((n_sp, capacity, model), bf16),
            pltpu.VMEM((n_sp, n_tp, capacity, model), bf16),
            pltpu.VMEM((n_sp // 2 * n_tp * capacity, f_width), bf16),
            pltpu.VMEM((2, n_y, n_sp, capacity, model), bf16),
            pltpu.VMEM((n_y, n_sp, capacity, model), bf16),
            pltpu.VMEM((n_y, n_sp, capacity, model), bf16),
            pltpu.VMEM((n_y, n_sp, capacity, model), bf16),
            pltpu.VMEM((n_sp, capacity, model), bf16),
            pltpu.VMEM((n_sp, capacity, model), bf16),
            pltpu.VMEM(out_weight.shape, bf16),
            pltpu.VMEM(expert_gate.shape[1:], bf16),
            pltpu.VMEM(expert_up.shape[1:], bf16),
            pltpu.VMEM(expert_down.shape[1:], bf16),
            dma((4,)),
            dma((n_sp,)),
            dma((n_sp,)),
            dma((n_sp,)),
            dma((n_sp,)),
            dma((n_tp,)),
            dma((n_tp,)),
            dma((n_sp,)),
            dma((n_sp, n_tp)),
            dma((n_sp, n_y)),
            dma((n_sp, n_y)),
            dma((2,)),
            dma((2,)),
            dma((n_sp, n_y)),
            dma((n_sp, n_y)),
            dma((n_sp,)),
            dma((n_sp,)),
        ],
        compiler_params=pltpu.CompilerParams(
            collective_id=0, has_side_effects=True, vmem_limit_bytes=56 * 1024 * 1024
        ),
    )(
        query_proj,
        projected_key_heads,
        projected_value_heads,
        head_frequency(),
        query_gain.reshape(1, -1),
        key_norm_gain.reshape(1, -1),
        x_resid,
        ffn_gain.reshape(1, -1),
        routing.T,
        route_scores.T,
        out_weight,
        expert_gate,
        expert_up,
        expert_down,
    ).astype(bf16)


def solution(mesh):
    in_specs = (
        P(("sp", "tp"), None),
        P("sp", "tp"),
        P("sp", "tp"),
        P("sp", "tp"),
        P(),
        P(),
        P("tp", None),
        P(),
        P(("sp", "tp"), None),
        P(("sp", "tp"), None),
        P("sp", None, "tp"),
        P("sp", None, "tp"),
        P("sp", "tp", None),
    )
    out_specs = P(("sp", "tp"), None)
    return jax.shard_map(local, mesh=mesh, in_specs=in_specs, out_specs=out_specs, check_vma=False)
```

profile of v0, /device:TPU:0, one launch (start us, length us, event | category | flops | bytes accessed | tf_op | source)
XLA Modules:
  0.0 77.9 jit_solution(5236808957680586493)
XLA Ops:
  0.0 76.2 %shard_map.136 = f32[32,2048]{1,0:T(8,128)} custom-call(bf16[128,512]{1,0:T(8,128)(2,1)} %q_ref.1, bf16[128,256]{1,0:T(8,128)(2,1)} %k_ref.1, bf16[128,256]{1,0:T(8,128)(2,1)} %v_ref.1, f32[1,128]{1,0:T(1,128)} %constant.2.clone.freq_ref, f32[1,128]{1,0:T(1,128)} %bitcast.8, f32[1,128]{1,0:T(1,128)} %bitcast.9, bf16[32,2048]{1,0:T(8,128)(2,1)} %x_ref.1, ...), custom_call_target="tpu_custom_call" | custom-call | tf_op jit(solution)/shard_map/pallas_call | solution.py:641
  76.2 1.6 %convert_element_type.3 = bf16[32,2048]{1,0:T(8,128)(2,1)} convert(f32[32,2048]{1,0:T(8,128)} %shard_map.136) | non-fusion elementwise | flops 65536 | bytes 393216 | tf_op jit(solution)/shard_map/convert_element_type | solution.py:703
where the time goes:
time: 78.2 us; the launch traced here: 77.9 us
  Pallas kernels  76.2 us (97%)
  other arithmetic  1.62 us (2%)
    pallas_call x1, Pallas kernels, local(): pl.pallas_call(functools.partial(layer_kernel, n_sp, n_tp, capacity), out...  76.2 us
    convert_element_type x1, other arithmetic, local(): return pl.pallas_call(functools.partial(layer_kernel, n_sp, n_tp, capacit...  1.62 us

commit v1 on v0

--- a/solution.py
+++ b/solution.py
@@ -213,18 +213,41 @@
 
 
 def hop_order(count):
-    half, quarter = count // 2, count // 4
-    near, far = list(range(half)), list(range(half, count))
-    return near[:quarter] + far + near[quarter:]
+    half = count // 2
+    near, far = list(range(2, half)), list(range(half, count))
+    order = [0, 1, far.pop(0)]
+    while near or far:
+        for pool in (far, near, far):
+            if pool:
+                order.append(pool.pop(0))
+    return order
+
+
+def group_edges(count):
+    return [0, 3 * count // 8, 6 * count // 8, count]
 
 
 def layer_kernel(
     n_sp,
     n_tp,
     capacity,
+    q_hbm,
+    k_hbm,
+    v_hbm,
+    freq_hbm,
+    qg_hbm,
+    kg_hbm,
+    x_hbm,
+    fg_hbm,
+    route_hbm,
+    score_hbm,
+    ow_hbm,
+    wg_hbm,
+    wu_hbm,
+    wd_hbm,
+    out_ref,
     q_ref,
     k_ref,
-    v_ref,
     freq_ref,
     qg_ref,
     kg_ref,
@@ -232,17 +255,15 @@
     fg_ref,
     route_ref,
     score_ref,
-    ow_hbm,
-    wg_hbm,
-    wu_hbm,
-    wd_hbm,
-    out_ref,
     kbuf,
     vbuf,
     qs,
     att,
     part,
+    prx,
+    psum,
     rsbuf,
+    direct,
     mid,
     disp,
     rows,
@@ -257,30 +278,23 @@
     wg,
     wu,
     wd,
+    in_sem,
     w_sem,
-    k_s,
+    s_sem,
     k_r,
-    v_s,
     v_r,
-    rs_s,
+    a_r,
     rs_r,
-    d_s,
-    rows_r,
-    y_s,
-    c_s,
-    e_s,
+    g_r,
+    d_r,
+    y_r,
+    c_r,
     e_r,
-    p_s,
     p_r,
-    b_s,
     b_r,
 ):
     s = lax.axis_index("sp")
     t = lax.axis_index("tp")
-    n_x = math.isqrt(n_sp // 2)
-    if n_x == 0 or n_sp % n_x:
-        n_x = 1
-    n_z = n_sp // n_x
     n_y = n_tp // 2
     y, c = t // 2, t % 2
     core_peer = (s, y * 2 + 1 - c)
@@ -291,58 +305,113 @@
     groups = q_heads // kv_heads
     own, model = x_ref.shape
     f_width = wg.shape[1]
-    pending = []
-
-    def send(src, dst, send_sem, recv_sem, device):
-        copy = rdma(src, dst, send_sem, recv_sem, device)
-        copy.start()
-        pending.append(copy)
+    tile = min(512, model)
+    tiles = model // tile
+    bits = [1 << i for i in range(n_sp.bit_length() - 1)]
+    sent = [0] * 3
+    edges = group_edges(n_sp)
+
+    def send(stage, src, dst, recv_sem, device):
+        rdma(src, dst, s_sem.at[stage], recv_sem, device).start()
+        sent[stage] += math.prod(src.shape)
 
     def arrive(dst, recv_sem):
         rdma(dst, dst, recv_sem, recv_sem, core_peer).wait_recv()
 
+    barrier = pltpu.get_barrier_semaphore()
+    for bit in bits:
+        pl.semaphore_signal(barrier, inc=1, device_id=(flip(s, bit), t), device_id_type=MESH)
+    for d in range(1, n_tp):
+        pl.semaphore_signal(barrier, inc=1, device_id=(s, (t + d) % n_tp), device_id_type=MESH)
+
+    inputs = {}
+    for name, src, dst in (
+        ("k", k_hbm, k_ref),
+        ("freq", freq_hbm, freq_ref),
+        ("kg", kg_hbm, kg_ref),
+        ("qg", qg_hbm, qg_ref),
+        ("q", q_hbm, q_ref),
+        ("route", route_hbm, route_ref),
+        ("score", score_hbm, score_ref),
+        ("x", x_hbm, x_ref),
+        ("fg", fg_hbm, fg_ref),
+    ):
+        inputs[name] = pltpu.make_async_copy(src, dst, in_sem.at[len(inputs)])
+        inputs[name].start()
+    value_copies = []
+    for h in range(kv_heads):
+        cols = slice(h * HEAD_WIDTH, (h + 1) * HEAD_WIDTH)
+        copy = pltpu.make_async_copy(
+            v_hbm.at[:, cols], vbuf.at[h, 0], in_sem.at[len(inputs) + h]
+        )
+        copy.start()
+        value_copies.append(copy)
     weight_copies = [
         pltpu.make_async_copy(ow_hbm, ow, w_sem.at[0]),
         pltpu.make_async_copy(wg_hbm.at[0], wg, w_sem.at[1]),
         pltpu.make_async_copy(wu_hbm.at[0], wu, w_sem.at[2]),
         pltpu.make_async_copy(wd_hbm.at[0], wd, w_sem.at[3]),
     ]
-    for copy in weight_copies:
-        copy.start()
-
-    barrier = pltpu.get_barrier_semaphore()
-    for d in range(1, n_sp):
-        pl.semaphore_signal(barrier, inc=1, device_id=((s + d) % n_sp, t), device_id_type=MESH)
-    for d in range(1, n_tp):
-        pl.semaphore_signal(barrier, inc=1, device_id=(s, (t + d) % n_tp), device_id_type=MESH)
 
     table = (seq_rows, HEAD_WIDTH)
     place = lax.broadcasted_iota(jnp.int32, table, 0) + s * seq_rows
     column = lax.broadcasted_iota(jnp.int32, table, 1)
     step = jnp.where(column < HEAD_WIDTH // 2, place // GRID_W, place % GRID_W)
+    inputs["freq"].wait()
     angles = step.astype(jnp.float32) * freq_ref[...]
     cosine, sine = jnp.cos(angles), jnp.sin(angles)
     sine = jnp.where(column % (HEAD_WIDTH // 2) < HEAD_WIDTH // 4, -sine, sine)
+    inputs["kg"].wait()
+    inputs["k"].wait()
     for h in range(kv_heads):
         cols = slice(h * HEAD_WIDTH, (h + 1) * HEAD_WIDTH)
-        kbuf[0, :, cols] = turn_head(k_ref[:, cols].astype(jnp.float32), kg_ref[...], cosine, sine)
-    pl.semaphore_wait(barrier, n_sp - 1 + n_tp - 1)
-
-    for slot in list(range(1, n_x)) + list(range(n_x, n_sp, n_x)):
-        send(kbuf.at[0], kbuf.at[slot], k_s.at[slot], k_r.at[slot], (flip(s, slot), t))
-
-    def send_values(slot):
-        send(v_ref, vbuf.at[slot], v_s.at[slot], v_r.at[slot], (flip(s, slot), t))
-
-    for slot in range(1, n_x):
-        send_values(slot)
-    vbuf[0] = v_ref[...]
+        kbuf[h, 0] = turn_head(k_ref[:, cols].astype(jnp.float32), kg_ref[...], cosine, sine)
+    pl.semaphore_wait(barrier, len(bits) + n_tp - 1)
+
+    def hop_bit(kind, slot):
+        return 2 if kind and slot == 3 else slot & -slot
+
+    kinds = ((kbuf, k_r), (vbuf, v_r))
+
+    def offer(kind, h, slot):
+        buf, r_sem = kinds[kind]
+        bit = hop_bit(kind, slot)
+        send(0, buf.at[h, slot ^ bit], buf.at[h, slot], r_sem.at[h, slot], (flip(s, bit), t))
+
+    settled = set()
+
+    def got(kind, h, slot):
+        if (kind, h, slot) not in settled:
+            settled.add((kind, h, slot))
+            buf, r_sem = kinds[kind]
+            arrive(buf.at[h, slot], r_sem.at[h, slot])
+
+    def pass_on(kind, h, slot):
+        got(kind, h, slot)
+        for child in range(n_sp - 1, slot, -1):
+            if child ^ hop_bit(kind, child) == slot:
+                offer(kind, h, child)
+
+    for h in range(kv_heads):
+        for bit in reversed(bits):
+            offer(0, h, bit)
+    for copy in value_copies:
+        copy.wait()
+    for bit in (bits[0], bits[-1]):
+        for h in range(kv_heads):
+            offer(1, h, bit)
+    inputs["qg"].wait()
+    inputs["q"].wait()
+    for copy in weight_copies:
+        copy.start()
     for h in range(q_heads):
         cols = slice(h * HEAD_WIDTH, (h + 1) * HEAD_WIDTH)
         kv, member = h // groups, h % groups
         qs[kv, member * seq_rows : (member + 1) * seq_rows, :] = turn_head(
             q_ref[:, cols].astype(jnp.float32), qg_ref[...], cosine, sine
         )
+    inputs["route"].wait()
+    inputs["score"].wait()
     total_slots = n_sp * capacity
     slot_at = lax.broadcasted_iota(jnp.int32, (total_slots, own), 0)
     slot_place = slot_at // capacity
@@ -369,29 +438,30 @@
     combiner = picked * jnp.where(first_hit, share[0:1, :], share[1:2, :])
     picker = picked.astype(jnp.bfloat16)
 
-    for buf, s_sem, r_sem in ((kbuf, k_s, k_r), (vbuf, v_s, v_r)):
-        for dz in range(1, n_z):
-            slot = dz * n_x
-            arrive(buf.at[slot], r_sem.at[slot])
-            for dx in range(1, n_x):
-                send(
-                    buf.at[slot],
-                    buf.at[slot + dx],
-                    s_sem.at[slot + dx],
-                    r_sem.at[slot + dx],
-                    (flip(s, dx), t),
-                )
-            if buf is kbuf:
-                send_values(slot)
-    for slot in range(n_sp):
-        if slot % n_x:
-            arrive(kbuf.at[slot], k_r.at[slot])
+    singles = [bit for bit in reversed(bits) if bit > 1]
+    deeper = [m for m in range(n_sp) if m % 2 == 0 and m & (m - 1)]
+    for h in range(kv_heads):
+        for bit in singles:
+            pass_on(0, h, bit)
+    for h in range(kv_heads):
+        pass_on(1, h, bits[-1])
+        for slot in deeper:
+            pass_on(0, h, slot)
+    for bit in bits[1:-1]:
+        for h in range(kv_heads):
+            offer(1, h, bit)
+    for h in range(kv_heads):
+        for slot in deeper:
+            pass_on(1, h, slot)
+    for h in range(kv_heads):
+        pass_on(1, h, 1)
     keys_all = n_sp * seq_rows
     score_scale = HEAD_WIDTH ** (-0.5)
     heads_done = []
     for kv in range(kv_heads):
-        cols = slice(kv * HEAD_WIDTH, (kv + 1) * HEAD_WIDTH)
-        keys = kbuf[:, :, cols].reshape(keys_all, HEAD_WIDTH)
+        for slot in range(1, n_sp):
+            got(0, kv, slot)
+        keys = kbuf[kv].reshape(keys_all, HEAD_WIDTH)
         scores = (
             lax.dot_general(
                 qs[kv], keys, (((1,), (1,)), ((), ())), preferred_element_type=jnp.float32
@@ -401,12 +471,10 @@
         weights = jnp.exp(scores - jnp.max(scores, axis=-1, keepdims=True))
         total = jnp.sum(weights, axis=-1, keepdims=True)
         heads_done.append((weights.astype(jnp.bfloat16), total))
-    for slot in range(n_sp):
-        if slot % n_x:
-            arrive(vbuf.at[slot], v_r.at[slot])
     for kv in range(kv_heads):
-        cols = slice(kv * HEAD_WIDTH, (kv + 1) * HEAD_WIDTH)
-        values = vbuf[:, :, cols].reshape(keys_all, HEAD_WIDTH)
+        for slot in range(1, n_sp):
+            got(1, kv, slot)
+        values = vbuf[kv].reshape(keys_all, HEAD_WIDTH)
         weights, total = heads_done[kv]
         mixed = jnp.dot(weights, values, preferred_element_type=jnp.float32) / total
         for member in range(groups):
@@ -416,28 +484,69 @@
             ].astype(jnp.bfloat16)
 
     weight_copies[0].wait()
-    tile = min(512, model)
-    for j in range(model // tile):
-        cols = slice(j * tile, (j + 1) * tile)
-        part[:, :, cols] = (
+    def project(cols):
+        product = (
             jnp.dot(att[...], ow[:, cols], preferred_element_type=jnp.float32)
             .astype(jnp.bfloat16)
-            .reshape(n_tp, own, tile)
+            .reshape(n_y, 2, own, -1)
         )
-    for d in range(n_tp - 1, 0, -1):
-        peer = flip(t, d)
-        send(part.at[peer], rsbuf.at[d], rs_s.at[d], rs_r.at[d], (s, peer))
-    summed = part[t].astype(jnp.float32)
-    for d in range(1, n_tp):
-        arrive(rsbuf.at[d], rs_r.at[d])
-        summed = summed + rsbuf[d].astype(jnp.float32)
-    middle = x_ref[...].astype(jnp.float32) + summed.astype(jnp.bfloat16).astype(jnp.float32)
-    mid[...] = middle
-    normed = (
-        middle
-        * lax.rsqrt(jnp.mean(middle * middle, axis=-1, keepdims=True) + NORM_EPS)
-        * fg_ref[...]
-    ).astype(jnp.bfloat16)
+        for core in range(2):
+            part[core, :, :, cols] = product[:, core]
+
+    def swap(j):
+        cols = slice(j * tile, (j + 1) * tile)
+        send(0, part.at[1 - c, :, :, cols], prx.at[:, :, cols], a_r.at[j], core_peer)
+
+    project(slice(0, tile))
+    cols = slice(0, tile)
+    for dy in range(1, n_y):
+        far = (y + dy) % n_y
+        for core in range(2):
+            send(
+                0,
+                part.at[(c + core) % 2, far, :, cols],
+                direct.at[dy, core, :, :],
+                g_r.at[dy - 1, core],
+                (s, far * 2 + (c + core) % 2),
+            )
+    project(slice(tile, model))
+    for j in range(1, tiles):
+        swap(j)
+    swap(0)
+    for j in range(1, tiles):
+        cols = slice(j * tile, (j + 1) * tile)
+        arrive(prx.at[:, :, cols], a_r.at[j])
+        for dy in range(1, n_y):
+            far = (y + dy) % n_y
+            psum[dy, :, cols] = (
+                part[c, far, :, cols].astype(jnp.float32) + prx[far, :, cols].astype(jnp.float32)
+            ).astype(jnp.bfloat16)
+            send(
+                0,
+                psum.at[dy, :, cols],
+                rsbuf.at[dy, :, cols],
+                rs_r.at[j, dy - 1],
+                (s, far * 2 + c),
+            )
+    arrive(prx.at[:, :, slice(0, tile)], a_r.at[0])
+    inputs["x"].wait()
+    inputs["fg"].wait()
+    squares = jnp.zeros((own, 1), jnp.float32)
+    for j in range(tiles):
+        cols = slice(j * tile, (j + 1) * tile)
+        summed = part[c, y, :, cols].astype(jnp.float32) + prx[y, :, cols].astype(jnp.float32)
+        for dy in range(1, n_y):
+            if j:
+                arrive(rsbuf.at[dy, :, cols], rs_r.at[j, dy - 1])
+                summed = summed + rsbuf[dy, :, cols].astype(jnp.float32)
+            else:
+                for core in range(2):
+                    arrive(direct.at[dy, core, :, :], g_r.at[dy - 1, core])
+                    summed = summed + direct[dy, core].astype(jnp.float32)
+        middle = x_ref[:, cols].astype(jnp.float32) + summed.astype(jnp.bfloat16).astype(jnp.float32)
+        mid[:, cols] = middle
+        squares = squares + jnp.sum(middle * middle, axis=-1, keepdims=True)
+    normed = (mid[...] * lax.rsqrt(squares / model + NORM_EPS) * fg_ref[...]).astype(jnp.bfloat16)
     chosen = (
         jnp.dot(picker, normed, preferred_element_type=jnp.float32)
         .astype(jnp.bfloat16)
@@ -448,143 +557,125 @@
     def dispatch(k):
         send(disp.at[k], rows.at[k, t], d_s.at[k], rows_r.at[k, t], (flip(s, order[k]), t))
 
-    window = n_sp // 2
-    for k in range(1, window):
-        dispatch(k)
-    rows[0, t] = chosen[0]
+    def dispatch(k):
+        send(1, disp.at[k], rows.at[k, c, y], d_r.at[k], (flip(s, order[k]), t))
 
     def forward(k):
         if k:
-            arrive(rows.at[k, t], rows_r.at[k, t])
+            arrive(rows.at[k, c, y], d_r.at[k])
         for dy in range(1, n_y):
             peer = ((y + dy) % n_y) * 2 + c
-            send(rows.at[k, t], rows.at[k, t], y_s.at[k, dy], rows_r.at[k, t], (s, peer))
-        send(rows.at[k, t], rows.at[k, t], c_s.at[k, 0], rows_r.at[k, t], core_peer)
+            send(1, rows.at[k, c, y], rows.at[k, c, y], y_r.at[k, dy - 1], (s, peer))
+        swap_rows(k, y)
+
+    def swap_rows(k, source):
+        group = sum(k >= edge for edge in edges[1:-1])
+        send(1, rows.at[k, c, source], rows.at[k, c, source], c_r.at[group], core_peer)
 
     def relay(k):
         for dy in range(1, n_y):
-            source = ((y + n_y - dy) % n_y) * 2 + c
-            arrive(rows.at[k, source], rows_r.at[k, source])
-            send(
-                rows.at[k, source],
-                rows.at[k, source],
-                c_s.at[k, dy],
-                rows_r.at[k, source],
-                core_peer,
-            )
-
-    def settle(k):
-        for dy in range(n_y):
-            source = ((y + n_y - dy) % n_y) * 2 + 1 - c
-            arrive(rows.at[k, source], rows_r.at[k, source])
-
-    n_groups = 2
-    group = n_sp // n_groups
-    group_rows = group * n_tp * capacity
-
-    def give_pair(g):
-        ks = pl.ds(g * group, group)
-        send(eo.at[1 - c, :, ks], cor.at[:, ks], e_s.at[g], e_r.at[g], core_peer)
-
-    def sum_pair(k):
+            source = (y + n_y - dy) % n_y
+            arrive(rows.at[k, c, source], y_r.at[k, dy - 1])
+            swap_rows(k, source)
+
+    def settle(g):
+        arrive(rows.at[edges[g] : edges[g + 1], 1 - c], c_r.at[g])
+
+    def span(g, j):
+        return slice(edges[g], edges[g + 1]), slice(j * tile, (j + 1) * tile)
+
+    def give_pair(g, j):
+        ks, cols = span(g, j)
+        send(2, eo.at[1 - c, :, ks, :, cols], cor.at[:, ks, :, cols], e_r.at[g, j], core_peer)
+
+    def sum_pair(g, j):
+        ks, cols = span(g, j)
+        arrive(cor.at[:, ks, :, cols], e_r.at[g, j])
         for dy in range(1, n_y):
             far = (y + dy) % n_y
-            pair[dy, k] = (
-                eo[c, far, k].astype(jnp.float32) + cor[far, k].astype(jnp.float32)
+            pair[dy, ks, :, cols] = (
+                eo[c, far, ks, :, cols].astype(jnp.float32) + cor[far, ks, :, cols].astype(jnp.float32)
             ).astype(jnp.bfloat16)
-            send(pair.at[dy, k], yrec.at[dy, k], p_s.at[k, dy], p_r.at[k, dy], (s, far * 2 + c))
-
-    def start_pairs(g, slots):
-        arrive(cor.at[:, pl.ds(g * group, group)], e_r.at[g])
-        for k in slots[:2]:
-            sum_pair(k)
-
-    def return_next(i, slots):
-        give_back(slots[i])
-        if i + 2 < len(slots):
-            sum_pair(slots[i + 2])
-
-    def give_back(k):
-        whole = eo[c, y, k].astype(jnp.float32) + cor[y, k].astype(jnp.float32)
+            send(
+                2,
+                pair.at[dy, ks, :, cols],
+                yrec.at[dy, ks, :, cols],
+                p_r.at[g * tiles + j, dy - 1],
+                (s, far * 2 + c),
+            )
+
+    def give_back(g, j):
+        ks, cols = span(g, j)
+        whole = eo[c, y, ks, :, cols].astype(jnp.float32) + cor[y, ks, :, cols].astype(jnp.float32)
         for dy in range(1, n_y):
-            arrive(yrec.at[dy, k], p_r.at[k, dy])
-            whole = whole + yrec[dy, k].astype(jnp.float32)
-        if k == 0:
-            ret[0] = whole.astype(jnp.bfloat16)
-        else:
-            res[k] = whole.astype(jnp.bfloat16)
-            send(res.at[k], ret.at[k], b_s.at[k], b_r.at[k], (flip(s, order[k]), t))
+            arrive(yrec.at[dy, ks, :, cols], p_r.at[g * tiles + j, dy - 1])
+            whole = whole + yrec[dy, ks, :, cols].astype(jnp.float32)
+        res[ks, :, cols] = whole.astype(jnp.bfloat16)
+        for k in range(edges[g], edges[g + 1]):
+            if k:
+                send(
+                    2, res.at[k, :, cols], ret.at[k, :, cols], b_r.at[j], (flip(s, order[k]), t)
+                )
+
+    def run(hooks, name):
+        do(*hooks.get(name, ()))
 
     def experts(g, hooks):
-        hooks = list(hooks)
-        block = rows[g * group : (g + 1) * group].reshape(group_rows, model)
+        low, high = edges[g], edges[g + 1]
+        group_rows = (high - low) * n_tp * capacity
+        block = rows[low:high].reshape(group_rows, model)
         f_tile = min(256, f_width)
         for j in range(f_width // f_tile):
             cols = slice(j * f_tile, (j + 1) * f_tile)
             gate = jnp.dot(block, wg[:, cols], preferred_element_type=jnp.float32)
             up = jnp.dot(block, wu[:, cols], preferred_element_type=jnp.float32)
-            hid[:, cols] = (gate / (1.0 + jnp.exp(-gate)) * up).astype(jnp.bfloat16)
-            if hooks:
-                hooks.pop(0)()
+            hid[:group_rows, cols] = (gate / (1.0 + jnp.exp(-gate)) * up).astype(jnp.bfloat16)
+            run(hooks, f"gu{g}{j}")
         if g == 0:
             weight_copies[3].wait()
-        for j in range(model // tile):
+        for j in range(tiles):
             cols = slice(j * tile, (j + 1) * tile)
-            down = jnp.dot(hid[...], wd[:, cols], preferred_element_type=jnp.float32)
-            down = down.astype(jnp.bfloat16).reshape(group, n_y, 2, capacity, tile)
+            down = jnp.dot(hid[:group_rows, :], wd[:, cols], preferred_element_type=jnp.float32)
+            down = down.astype(jnp.bfloat16).reshape(high - low, 2, n_y, capacity, tile)
             for core in range(2):
                 for far in range(n_y):
-                    eo[core, far, g * group : (g + 1) * group, :, cols] = down[:, far, core]
-            if hooks:
-                hooks.pop(0)()
-        for hook in hooks:
-            hook()
-
-    for k in range(group):
-        forward(k)
-        if k:
-            dispatch(window + k - 1)
-    dispatch(n_sp - 1)
-    for k in range(group):
-        relay(k)
-    for k in range(group):
-        settle(k)
+                    eo[core, far, low:high, :, cols] = down[:, core, far]
+            give_pair(g, j)
+            run(hooks, f"dn{g}{j}")
+
+    steps = {"D": dispatch, "F": forward, "R": relay, "S": settle, "P": sum_pair, "G": give_back}
+
+    def do(*names):
+        for name in names:
+            steps[name[0]](*(int(d) for d in name[1:]))
+
+    rows[0, c, y] = chosen[0]
+    do("D2", "D3", "D1", "F0", "F1", "R0", "D4", "D5", "F2", "D6", "D7", "R1", "F3", "F4", "R2", "S0")
     weight_copies[1].wait()
     weight_copies[2].wait()
-    late = range(group, n_sp)
-    experts(
-        0,
-        [functools.partial(forward, k) for k in late] + [functools.partial(relay, k) for k in late],
-    )
-    give_pair(0)
-    for k in late:
-        settle(k)
-    nothing = lambda: None
-    early = list(range(group - 1, -1, -1))
-    experts(
-        1,
-        [functools.partial(start_pairs, 0, early), nothing, nothing, nothing]
-        + [functools.partial(return_next, i, early) for i in range(group)],
-    )
-    give_pair(1)
-    start_pairs(1, late)
-    for i in range(group):
-        return_next(i, late)
-    for k in range(1, n_sp):
-        arrive(ret.at[k], b_r.at[k])
+    experts(0, {"gu01": ("F5", "R4"), "gu03": ("R3", "F7"), "dn01": ("F6",), "dn02": ("P00", "R5"), "dn03": ("P01",)})
+    do("S1")
+    experts(1, {"gu10": ("P02", "P03"), "gu11": ("R7", "R6"), "gu13": ("G00",), "dn11": ("G01",), "dn12": ("P10",), "dn13": ("P11",)})
+    do("S2")
+    experts(2, {"gu20": ("P12", "P13", "G02", "G03"), "gu22": ("G10",), "dn20": ("G11",), "dn22": ("P20",), "dn23": ("P21", "G12")})
+    do("P22", "P23", "G13", "G20", "G21", "G22", "G23")
     high = combiner.astype(jnp.bfloat16)
     rest = combiner - high.astype(jnp.float32)
     middle_part = rest.astype(jnp.bfloat16)
     low = (rest - middle_part.astype(jnp.float32)).astype(jnp.bfloat16)
-    returned = ret[...].reshape(total_slots, model)
-    routed = jnp.zeros((own, model), jnp.float32)
-    for piece in (high, middle_part, low):
-        routed = routed + lax.dot_general(
-            piece, returned, (((0,), (0,)), ((), ())), preferred_element_type=jnp.float32
-        )
-    out_ref[...] = mid[...] + routed
-    for copy in pending:
-        copy.wait_send()
+    for j in range(tiles):
+        cols = slice(j * tile, (j + 1) * tile)
+        arrive(ret.at[1:, :, cols], b_r.at[j])
+        returned = jnp.concatenate([res[0:1, :, cols], ret[1:, :, cols]]).reshape(total_slots, tile)
+        routed = jnp.zeros((own, tile), jnp.float32)
+        for piece in (high, middle_part, low):
+            routed = routed + lax.dot_general(
+                piece, returned, (((0,), (0,)), ((), ())), preferred_element_type=jnp.float32
+            )
+        out_ref[:, cols] = (mid[:, cols] + routed).astype(jnp.bfloat16)
+    for stage, count in enumerate(sent):
+        shipped = wg.at[pl.ds(0, count // f_width)]
+        rdma(shipped, shipped, s_sem.at[stage], s_sem.at[stage], core_peer).wait_send()
 
 
 def head_frequency():
@@ -634,26 +725,41 @@
     groups = q_width // kv_width
     f_width = expert_gate.shape[2]
     n_y = n_tp // 2
+    tiles = model // min(512, model)
+    edges = group_edges(n_sp)
+    groups_all = len(edges) - 1
+    group_most = max(b - a for a, b in zip(edges, edges[1:]))
     bf16 = jnp.bfloat16
     dma = pltpu.SemaphoreType.DMA
-    vmem = pl.BlockSpec(memory_space=pltpu.VMEM)
     hbm = pl.BlockSpec(memory_space=pl.ANY)
     return pl.pallas_call(
         functools.partial(layer_kernel, n_sp, n_tp, capacity),
-        out_shape=jax.ShapeDtypeStruct((own, model), jnp.float32),
-        in_specs=[vmem] * 10 + [hbm] * 4,
-        out_specs=vmem,
+        out_shape=pltpu.VMEM((own, model), bf16),
+        in_specs=[hbm] * 14,
+        out_specs=pl.BlockSpec(memory_space=pltpu.VMEM),
         scratch_shapes=[
-            pltpu.VMEM((n_sp, seq_rows, kv_width), bf16),
-            pltpu.VMEM((n_sp, seq_rows, kv_width), bf16),
+            pltpu.VMEM(query_proj.shape, bf16),
+            pltpu.VMEM(projected_key_heads.shape, bf16),
+            pltpu.VMEM((1, HEAD_WIDTH), jnp.float32),
+            pltpu.VMEM((1, HEAD_WIDTH), jnp.float32),
+            pltpu.VMEM((1, HEAD_WIDTH), jnp.float32),
+            pltpu.VMEM((own, model), bf16),
+            pltpu.VMEM((1, model), jnp.float32),
+            pltpu.VMEM((TOP, own), jnp.int32),
+            pltpu.VMEM((TOP, own), jnp.float32),
+            pltpu.VMEM((kv_heads, n_sp, seq_rows, HEAD_WIDTH), bf16),
+            pltpu.VMEM((kv_heads, n_sp, seq_rows, HEAD_WIDTH), bf16),
             pltpu.VMEM((kv_heads, groups * seq_rows, HEAD_WIDTH), bf16),
             pltpu.VMEM((seq_rows, q_width), bf16),
-            pltpu.VMEM((n_tp, own, model), bf16),
-            pltpu.VMEM((n_tp, own, model), bf16),
+            pltpu.VMEM((2, n_y, own, model), bf16),
+            pltpu.VMEM((n_y, own, model), bf16),
+            pltpu.VMEM((n_y, own, model), bf16),
+            pltpu.VMEM((n_y, own, model), bf16),
+            pltpu.VMEM((n_y, 2, own, model // tiles), bf16),
             pltpu.VMEM((own, model), jnp.float32),
             pltpu.VMEM((n_sp, capacity, model), bf16),
-            pltpu.VMEM((n_sp, n_tp, capacity, model), bf16),
-            pltpu.VMEM((n_sp // 2 * n_tp * capacity, f_width), bf16),
+            pltpu.VMEM((n_sp, 2, n_y, capacity, model), bf16),
+            pltpu.VMEM((group_most * n_tp * capacity, f_width), bf16),
             pltpu.VMEM((2, n_y, n_sp, capacity, model), bf16),
             pltpu.VMEM((n_y, n_sp, capacity, model), bf16),
             pltpu.VMEM((n_y, n_sp, capacity, model), bf16),
@@ -664,23 +770,20 @@
             pltpu.VMEM(expert_gate.shape[1:], bf16),
             pltpu.VMEM(expert_up.shape[1:], bf16),
             pltpu.VMEM(expert_down.shape[1:], bf16),
+            dma((9 + kv_heads,)),
             dma((4,)),
+            dma((3,)),
+            dma((kv_heads, n_sp)),
+            dma((kv_heads, n_sp)),
+            dma((tiles,)),
+            dma((tiles, n_y - 1)),
+            dma((n_y - 1, 2)),
             dma((n_sp,)),
-            dma((n_sp,)),
-            dma((n_sp,)),
-            dma((n_sp,)),
-            dma((n_tp,)),
-            dma((n_tp,)),
-            dma((n_sp,)),
-            dma((n_sp, n_tp)),
-            dma((n_sp, n_y)),
-            dma((n_sp, n_y)),
-            dma((2,)),
-            dma((2,)),
-            dma((n_sp, n_y)),
-            dma((n_sp, n_y)),
-            dma((n_sp,)),
-            dma((n_sp,)),
+            dma((n_sp, n_y - 1)),
+            dma((groups_all,)),
+            dma((groups_all, tiles)),
+            dma((groups_all * tiles, n_y - 1)),
+            dma((tiles,)),
         ],
         compiler_params=pltpu.CompilerParams(
             collective_id=0, has_side_effects=True, vmem_limit_bytes=56 * 1024 * 1024
@@ -700,7 +803,7 @@
         expert_gate,
         expert_up,
         expert_down,
-    ).astype(bf16)
+    )
 
 
 def solution(mesh):

time: 78.2 us -> 65.1 us (0.83)
  Pallas kernels: 76.2 us -> 64.3 us
  other arithmetic: 1.62 us -> 0 us
    pallas_call x1, Pallas kernels: 76.2 us -> 64.3 us  [local(): pl.pallas_call(functools.partial(layer_kernel, n_sp, n_tp, capacity), out...]
    convert_element_type x1 -> x0, other arithmetic: 1.62 us -> none  [local(): return pl.pallas_call(functools.partial(layer_kernel, n_sp, n_tp, capacit...]
where the time goes in v1:
time: 65.1 us; the launch traced here: 65 us
  Pallas kernels  64.3 us (99%)
  local copies, waits for them, and re-layouts  0.66 us (1%)
    pallas_call x1, Pallas kernels, local(): pl.pallas_call(functools.partial(layer_kernel, n_sp, n_tp, capacity), out...  64.3 us

profile of v1, /device:TPU:0, one launch (start us, length us, event | category | flops | bytes accessed | tf_op | source)
XLA Modules:
  0.0 65.0 jit_solution(14472127908975201570)
XLA Ops:
  0.0 64.3 %shard_map.136 = bf16[32,2048]{1,0:T(8,128)(2,1)S(1)} custom-call(bf16[128,512]{1,0:T(8,128)(2,1)} %q_hbm.1, bf16[128,256]{1,0:T(8,128)(2,1)} %k_hbm.1, bf16[128,256]{1,0:T(8,128)(2,1)} %v_hbm.1, f32[1,128]{1,0:T(1,128)} %constant.2.clone.freq_hbm, f32[1,128]{1,0:T(1,128)} %bitcast.8, f32[1,128]{1,0:T(1,128)} %bitcast.9, bf16[32,2048]{1,0:T(8,128)(2,1)} %x_hbm.1, ...), custom_call_target="tpu_custom_call" | custom-call | tf_op jit(solution)/shard_map/pallas_call | solution.py:735
  64.3 0.7 %copy.16 = bf16[32,2048]{1,0:T(8,128)(2,1)} copy(bf16[32,2048]{1,0:T(8,128)(2,1)S(1)} %shard_map.136) | data formatting | bytes 262144

commit v2 on v1

--- a/solution.py
+++ b/solution.py
@@ -19,6 +19,8 @@
 NORM_EPS = 1e-06
 ROPE_BASE = 10000.0
 NEG_LARGE = -1e30
+PLAN_SPOTS = 8
+PLAN_TILES = 4
 
 
 def rms_scale(values, norm_gain):
@@ -213,14 +215,28 @@
 
 
 def hop_order(count):
-    half = count // 2
-    near, far = list(range(2, half)), list(range(half, count))
-    order = [0, 1, far.pop(0)]
+    half, quarter = count // 2, count // 4
+    near, far = list(range(quarter, half)), list(range(half, count))
+    far = far[1:] + far[:1]
+    order = list(range(quarter)) + [far.pop(0)]
     while near or far:
         for pool in (far, near, far):
             if pool:
                 order.append(pool.pop(0))
     return order
+
+
+def hop_bit(kind, slot):
+    return {3: 2, 6: 6}.get(slot, slot & -slot) if kind else slot & -slot
+
+
+def inner_slots(count, kind):
+    parents = {child ^ hop_bit(kind, child) for child in range(1, count)}
+    return sorted(parents - {0})
+
+
+def crossed_first(count):
+    return [k for k, hop in enumerate(hop_order(count)) if count // 4 <= hop < count // 2]
 
 
 def group_edges(count):
@@ -266,6 +282,7 @@
     direct,
     mid,
     disp,
+    via,
     rows,
     hid,
     eo,
@@ -287,6 +304,7 @@
     rs_r,
     g_r,
     d_r,
+    v2_r,
     y_r,
     c_r,
     e_r,
@@ -310,6 +328,7 @@
     bits = [1 << i for i in range(n_sp.bit_length() - 1)]
     sent = [0] * 3
     edges = group_edges(n_sp)
+    crossed = crossed_first(n_sp)
 
     def send(stage, src, dst, recv_sem, device):
         rdma(src, dst, s_sem.at[stage], recv_sem, device).start()
@@ -368,23 +387,28 @@
         kbuf[h, 0] = turn_head(k_ref[:, cols].astype(jnp.float32), kg_ref[...], cosine, sine)
     pl.semaphore_wait(barrier, len(bits) + n_tp - 1)
 
-    def hop_bit(kind, slot):
-        return 2 if kind and slot == 3 else slot & -slot
-
     kinds = ((kbuf, k_r), (vbuf, v_r))
 
     def offer(kind, h, slot):
         buf, r_sem = kinds[kind]
         bit = hop_bit(kind, slot)
-        send(0, buf.at[h, slot ^ bit], buf.at[h, slot], r_sem.at[h, slot], (flip(s, bit), t))
-
+        spot = inner[kind].index(slot) if slot in inner[kind] else len(inner[kind])
+        send(0, buf.at[h, slot ^ bit], buf.at[h, slot], r_sem.at[h, spot], (flip(s, bit), t))
+
+    inner = [inner_slots(n_sp, kind) for kind in range(2)]
     settled = set()
 
     def got(kind, h, slot):
         if (kind, h, slot) not in settled:
             settled.add((kind, h, slot))
             buf, r_sem = kinds[kind]
-            arrive(buf.at[h, slot], r_sem.at[h, slot])
+            arrive(buf.at[h, slot], r_sem.at[h, inner[kind].index(slot)])
+
+    def got_all(kind, h):
+        buf, r_sem = kinds[kind]
+        for slot in inner[kind]:
+            got(kind, h, slot)
+        arrive(buf.at[h, pl.ds(0, n_sp - 1 - len(inner[kind]))], r_sem.at[h, len(inner[kind])])
 
     def pass_on(kind, h, slot):
         got(kind, h, slot)
@@ -443,24 +467,27 @@
     for h in range(kv_heads):
         for bit in singles:
             pass_on(0, h, bit)
+        for slot in deeper:
+            offer(1, h, slot)
     for h in range(kv_heads):
+        if h == 0:
+            for bit in bits[1:-1]:
+                offer(1, h, bit)
         pass_on(1, h, bits[-1])
+        pass_on(1, h, 1)
         for slot in deeper:
             pass_on(0, h, slot)
-    for bit in bits[1:-1]:
-        for h in range(kv_heads):
-            offer(1, h, bit)
+        if h:
+            for bit in bits[1:-1]:
+                offer(1, h, bit)
     for h in range(kv_heads):
         for slot in deeper:
             pass_on(1, h, slot)
-    for h in range(kv_heads):
-        pass_on(1, h, 1)
     keys_all = n_sp * seq_rows
     score_scale = HEAD_WIDTH ** (-0.5)
     heads_done = []
     for kv in range(kv_heads):
-        for slot in range(1, n_sp):
-            got(0, kv, slot)
+        got_all(0, kv)
         keys = kbuf[kv].reshape(keys_all, HEAD_WIDTH)
         scores = (
             lax.dot_general(
@@ -472,8 +499,7 @@
         total = jnp.sum(weights, axis=-1, keepdims=True)
         heads_done.append((weights.astype(jnp.bfloat16), total))
     for kv in range(kv_heads):
-        for slot in range(1, n_sp):
-            got(1, kv, slot)
+        got_all(1, kv)
         values = vbuf[kv].reshape(keys_all, HEAD_WIDTH)
         weights, total = heads_done[kv]
         mixed = jnp.dot(weights, values, preferred_element_type=jnp.float32) / total
@@ -557,26 +583,64 @@
     def dispatch(k):
         send(disp.at[k], rows.at[k, t], d_s.at[k], rows_r.at[k, t], (flip(s, order[k]), t))
 
+    halves = [slice(i * model // 2, (i + 1) * model // 2) for i in range(2)]
+
     def dispatch(k):
-        send(1, disp.at[k], rows.at[k, c, y], d_r.at[k], (flip(s, order[k]), t))
+        for i, cols in enumerate(halves):
+            send(
+                1,
+                disp.at[k, :, cols],
+                rows.at[k, c, y, :, cols],
+                d_r.at[k, i],
+                (flip(s, order[k]), t),
+            )
 
     def forward(k):
-        if k:
-            arrive(rows.at[k, c, y], d_r.at[k])
-        for dy in range(1, n_y):
-            peer = ((y + dy) % n_y) * 2 + c
-            send(1, rows.at[k, c, y], rows.at[k, c, y], y_r.at[k, dy - 1], (s, peer))
-        swap_rows(k, y)
-
-    def swap_rows(k, source):
+        for i, cols in enumerate(halves):
+            if k:
+                arrive(rows.at[k, c, y, :, cols], d_r.at[k, i])
+            for dy in range(1, n_y):
+                peer = ((y + dy) % n_y) * 2 + c
+                if k not in crossed:
+                    send(
+                        1,
+                        rows.at[k, c, y, :, cols],
+                        rows.at[k, c, y, :, cols],
+                        y_r.at[k, (dy - 1) * 2 + i],
+                        (s, peer),
+                    )
+            swap_rows(k, y, cols)
+
+    def swap_rows(k, source, cols):
         group = sum(k >= edge for edge in edges[1:-1])
-        send(1, rows.at[k, c, source], rows.at[k, c, source], c_r.at[group], core_peer)
+        send(
+            1, rows.at[k, c, source, :, cols], rows.at[k, c, source, :, cols], c_r.at[group], core_peer
+        )
 
     def relay(k):
         for dy in range(1, n_y):
             source = (y + n_y - dy) % n_y
-            arrive(rows.at[k, c, source], y_r.at[k, dy - 1])
-            swap_rows(k, source)
+            for i, cols in enumerate(halves):
+                arrive(rows.at[k, c, source, :, cols], y_r.at[k, (dy - 1) * 2 + i])
+                swap_rows(k, source, cols)
+
+    def early(k):
+        for dy in range(1, n_y):
+            peer = ((y + dy) % n_y) * 2 + c
+            send(1, disp.at[k], via.at[crossed.index(k), dy], v2_r.at[crossed.index(k), dy - 1], (s, peer))
+
+    def onward(k):
+        for dy in range(1, n_y):
+            source = (y + n_y - dy) % n_y
+            arrive(via.at[crossed.index(k), dy], v2_r.at[crossed.index(k), dy - 1])
+            for i, cols in enumerate(halves):
+                send(
+                    1,
+                    via.at[crossed.index(k), dy, :, cols],
+                    rows.at[k, c, source, :, cols],
+                    y_r.at[k, (dy - 1) * 2 + i],
+                    (flip(s, order[k]), t),
+                )
 
     def settle(g):
         arrive(rows.at[edges[g] : edges[g + 1], 1 - c], c_r.at[g])
@@ -643,22 +707,22 @@
             give_pair(g, j)
             run(hooks, f"dn{g}{j}")
 
-    steps = {"D": dispatch, "F": forward, "R": relay, "S": settle, "P": sum_pair, "G": give_back}
+    steps = {"D": dispatch, "F": forward, "R": relay, "S": settle, "E": early, "V": onward, "P": sum_pair, "G": give_back}
 
     def do(*names):
         for name in names:
             steps[name[0]](*(int(d) for d in name[1:]))
 
     rows[0, c, y] = chosen[0]
-    do("D2", "D3", "D1", "F0", "F1", "R0", "D4", "D5", "F2", "D6", "D7", "R1", "F3", "F4", "R2", "S0")
+    do("D2", "D3", "D1", "F0", "E4", "F1", "R0", "D5", "D6", "F2", "E7", "D4", "D7", "R1", "R2", "S0")
     weight_copies[1].wait()
     weight_copies[2].wait()
-    experts(0, {"gu01": ("F5", "R4"), "gu03": ("R3", "F7"), "dn01": ("F6",), "dn02": ("P00", "R5"), "dn03": ("P01",)})
-    do("S1")
-    experts(1, {"gu10": ("P02", "P03"), "gu11": ("R7", "R6"), "gu13": ("G00",), "dn11": ("G01",), "dn12": ("P10",), "dn13": ("P11",)})
+    experts(0, {"gu00": ("F3", "V4"), "gu01": ("V7",), "gu02": ("F5",), "dn00": ("R3", "F4"), "dn01": ("F6",), "dn03": ("R4", "P00")})
+    do("R5", "P01", "S1", "P02", "P03")
+    experts(1, {"gu13": ("R6", "F7"), "dn10": ("G00",), "dn11": ("R7",), "dn12": ("P10",), "dn13": ("P11", "G01")})
     do("S2")
-    experts(2, {"gu20": ("P12", "P13", "G02", "G03"), "gu22": ("G10",), "dn20": ("G11",), "dn22": ("P20",), "dn23": ("P21", "G12")})
-    do("P22", "P23", "G13", "G20", "G21", "G22", "G23")
+    experts(2, {"gu20": ("P12", "G02", "P13"), "gu21": ("G03",), "gu23": ("G10",), "dn21": ("G11",), "dn22": ("P20",), "dn23": ("P21",)})
+    do("P22", "G12", "P23", "G13", "G20", "G21", "G22", "G23")
     high = combiner.astype(jnp.bfloat16)
     rest = combiner - high.astype(jnp.float32)
     middle_part = rest.astype(jnp.bfloat16)
@@ -703,7 +767,12 @@
     own, model = x_resid.shape
     experts_all = n_sp * expert_gate.shape[0]
     capacity = max(2, 2 * own * TOP // experts_all)
-    if capacity % 16 or n_tp & (n_tp - 1) or n_sp & (n_sp - 1) or n_tp < 2 or n_sp < 4 or expert_gate.shape[0] != 1:
+    planned = (
+        n_sp == PLAN_SPOTS
+        and model == PLAN_TILES * min(512, model)
+        and expert_gate.shape[2] == PLAN_TILES * min(256, expert_gate.shape[2])
+    )
+    if capacity % 16 or n_tp & (n_tp - 1) or n_tp < 2 or not planned or expert_gate.shape[0] != 1:
         return local_plain(
             x_resid,
             query_proj,
@@ -758,6 +827,7 @@
             pltpu.VMEM((n_y, 2, own, model // tiles), bf16),
             pltpu.VMEM((own, model), jnp.float32),
             pltpu.VMEM((n_sp, capacity, model), bf16),
+            pltpu.VMEM((len(crossed_first(n_sp)), n_y, capacity, model), bf16),
             pltpu.VMEM((n_sp, 2, n_y, capacity, model), bf16),
             pltpu.VMEM((group_most * n_tp * capacity, f_width), bf16),
             pltpu.VMEM((2, n_y, n_sp, capacity, model), bf16),
@@ -773,13 +843,14 @@
             dma((9 + kv_heads,)),
             dma((4,)),
             dma((3,)),
-            dma((kv_heads, n_sp)),
-            dma((kv_heads, n_sp)),
+            dma((kv_heads, len(inner_slots(n_sp, 0)) + 1)),
+            dma((kv_heads, len(inner_slots(n_sp, 1)) + 1)),
             dma((tiles,)),
             dma((tiles, n_y - 1)),
             dma((n_y - 1, 2)),
-            dma((n_sp,)),
-            dma((n_sp, n_y - 1)),
+            dma((n_sp, 2)),
+            dma((len(crossed_first(n_sp)), n_y - 1)),
+            dma((n_sp, (n_y - 1) * 2)),
             dma((groups_all,)),
             dma((groups_all, tiles)),
             dma((groups_all * tiles, n_y - 1)),

time: 65.1 us -> 61.8 us (0.949)
  Pallas kernels: 64.3 us -> 61 us
    pallas_call x1, Pallas kernels: 64.3 us -> 61 us  [local(): pl.pallas_call(functools.partial(layer_kernel, n_sp, n_tp, capacity), out...]
where the time goes in v2:
time: 61.8 us; the launch traced here: 61.7 us
  Pallas kernels  61 us (99%)
  local copies, waits for them, and re-layouts  0.66 us (1%)
    pallas_call x1, Pallas kernels, local(): pl.pallas_call(functools.partial(layer_kernel, n_sp, n_tp, capacity), out...  61 us

profile of v2, /device:TPU:0, one launch (start us, length us, event | category | flops | bytes accessed | tf_op | source)
XLA Modules:
  0.0 61.7 jit_solution(17379834652692492919)
XLA Ops:
  0.0 61.0 %shard_map.136 = bf16[32,2048]{1,0:T(8,128)(2,1)S(1)} custom-call(bf16[128,512]{1,0:T(8,128)(2,1)} %q_hbm.1, bf16[128,256]{1,0:T(8,128)(2,1)} %k_hbm.1, bf16[128,256]{1,0:T(8,128)(2,1)} %v_hbm.1, f32[1,128]{1,0:T(1,128)} %constant.2.clone.freq_hbm, f32[1,128]{1,0:T(1,128)} %bitcast.8, f32[1,128]{1,0:T(1,128)} %bitcast.9, bf16[32,2048]{1,0:T(8,128)(2,1)} %x_hbm.1, ...), custom_call_target="tpu_custom_call" | custom-call | tf_op jit(solution)/shard_map/pallas_call | solution.py:804
  61.0 0.7 %copy.16 = bf16[32,2048]{1,0:T(8,128)(2,1)} copy(bf16[32,2048]{1,0:T(8,128)(2,1)S(1)} %shard_map.136) | data formatting | bytes 262144
